TPU v7x, 512 devices: a whole 4x4x16 slice. The times are simulated.
512 devices in a mesh: sp: 16 (over z), fs: 4 (over y), tp: 8 (over x, core).
Axes of the slice: x: 4, y: 4, z: 16, core: 2. Of those that a mesh axis runs over, the one named last changes fastest.
Arguments:
- inputs: bfloat16 [4, 2048, 2048], P('fs', 'sp'), may hold values from -6 to 6
- norm_gain: float32 [2048], replicated, may hold values from 0.1 to 1.9
- w_gate: bfloat16 [2048, 2048], P(('sp', 'fs'), 'tp'), may hold values from -0.125 to 0.125
- w_input: bfloat16 [2048, 2048], P(('sp', 'fs'), 'tp'), may hold values from -0.125 to 0.125
- w_bkey: bfloat16 [2048, 1024], P(('sp', 'fs'), 'tp'), may hold values from -0.125 to 0.125
- w_cquery: bfloat16 [2048, 1024], P(('sp', 'fs'), 'tp'), may hold values from -0.125 to 0.125
- w_step: bfloat16 [2048, 32], replicated, may hold values from -0.125 to 0.125
- conv_weight: float32 [4, 4096], replicated, may hold values from -2 to 2
- decay_rate: float32 [32], replicated, may hold values from 0 to 0.05, as said below
- decay_offset: float32 [4, 2048, 32], P('fs', 'sp', 'tp'), may hold values from -2 to 0
- ssd_gain: float32 [2048], replicated, may hold values from 0.1 to 1.9
- w_query: bfloat16 [2048, 2048], P(('sp', 'fs'), 'tp'), may hold values from -0.125 to 0.125
- w_key: bfloat16 [2048, 2048], P(('sp', 'fs'), 'tp'), may hold values from -0.125 to 0.125
- w_value: bfloat16 [2048, 2048], P(('sp', 'fs'), 'tp'), may hold values from -0.125 to 0.125
- stick_bias: float32 [16], replicated, may hold values from -12 to 0
- out_mixer: bfloat16 [2048, 2048], P('tp', ('sp', 'fs')), may hold values from -0.125 to 0.125
- out_attend: bfloat16 [2048, 2048], P('tp', ('sp', 'fs')), may hold values from -3.59375 to 3.59375
Outputs:
- mixed: bfloat16 [4, 2048, 2048], P('fs', ('sp', 'tp'))
Inputs may be any that keep to these rules, and one draw needn't show every extreme that they name: `decay_rate`: one positive rate for each head.
All inputs are finite; a program needn't handle non-finite values.
Results may differ from a plain program's by a relative error of at most 0.015.
Values may be sent and summed in bfloat16 or wider, within the bound.
No kernel may reach another device: no remote copies, remote signals or barrier semaphores. Data moves between devices by JAX's collectives and lax.ppermute only.
A program may use at most 64 MiB of HBM per device.

v0:
```python
import functools

import jax
import jax.numpy as jnp
from jax import lax
from jax.experimental import pallas as pl
from jax.experimental.pallas import tpu as pltpu
from jax.sharding import PartitionSpec as P


BLOCK = 128
CONV = 4
EPS = 1e-06
HALO = 16
ROWS = BLOCK + HALO
F32 = jnp.float32
BF16 = jnp.bfloat16
HIGH = lax.Precision.HIGHEST
NT = (((1,), (1,)), ((), ()))
TN = (((0,), (0,)), ((), ()))


def vmem(limit=48):
    return pltpu.CompilerParams(vmem_limit_bytes=limit * 1024 * 1024)


def iota(shape, dim):
    return lax.broadcasted_iota(jnp.int32, shape, dim)


def softplus(x):
    return jnp.maximum(x, 0.0) + jnp.log1p(jnp.exp(-jnp.abs(x)))


def silu(x):
    return x / (1.0 + jnp.exp(-x))


def pull(pairs, sems):
    copies = [pltpu.make_async_copy(src, dst, sems.at[i]) for i, (src, dst) in enumerate(pairs)]
    for copy in copies:
        copy.start()
    return copies


def shuffled(normed, f, g):
    lane = iota((normed.shape[0], 128), 1) // 32
    out = None
    for k in range(4):
        at = (4 * g + k) * 128
        piece = normed[:, at : at + 128]
        shift = ((k - f) * 32) % 128
        if shift:
            piece = pltpu.roll(piece, shift, 1)
        out = piece if out is None else jnp.where(lane == k, piece, out)
    return out.astype(BF16)


def normalised(x, gain):
    wide = x.astype(F32)
    scale = lax.rsqrt(jnp.mean(wide * wide, axis=-1, keepdims=True) + EPS)
    return (wide * scale * gain).astype(BF16)


def prep_kernel(*refs):
    x_hbm, gain_hbm, ws_hbm = refs[:3]
    sources = refs[3:12]
    xs_ref, step_ref, first_ref, second_ref = refs[12:16]
    x_ref, gain_ref, ws_ref, third_ref, sems, wsems = refs[16:]
    early = pull(((x_hbm.at[0], x_ref), (gain_hbm, gain_ref), (ws_hbm, ws_ref)), sems)
    pairs = []
    outs = (first_ref, second_ref, third_ref)
    at, which = 0, 0
    for n, src in enumerate(sources):
        if n in (4, 8):
            at, which = 0, which + 1
        pairs.append((src, outs[which].at[:, pl.ds(at, src.shape[1])]))
        at += src.shape[1]
    later = pull(pairs, wsems)
    for copy in early:
        copy.wait()
    normed = normalised(x_ref[...], gain_ref[...])
    step_ref[...] = softplus(
        lax.dot_general(ws_ref[...], normed, NT, preferred_element_type=F32)
    )
    wide = normed.astype(F32)
    for f in range(4):
        for g in range(4):
            xs_ref[f, 0:BLOCK, g * 128 : (g + 1) * 128] = shuffled(wide, f, g)
    for copy in later:
        copy.wait()
    for f in range(4):
        xs_ref[f, BLOCK:, 0:256] = third_ref[0:16, :]
        xs_ref[f, BLOCK:, 256:512] = third_ref[16:32, :]


def prep_call(inputs, gain, w_step_t, *arrays):
    rows, width = inputs.shape[1:]
    heads = w_step_t.shape[0]
    part = arrays[0].shape[0]
    widths = [sum(a.shape[1] for a in group) for group in (arrays[:4], arrays[4:8], arrays[8:])]
    hbm = pl.BlockSpec(memory_space=pltpu.HBM)
    return pl.pallas_call(
        prep_kernel,
        in_specs=[hbm] * 12,
        out_shape=(
            jax.ShapeDtypeStruct((4, rows + HALO, width // 4), BF16),
            jax.ShapeDtypeStruct((heads, rows), F32),
            jax.ShapeDtypeStruct((part, widths[0]), BF16),
            jax.ShapeDtypeStruct((part, widths[1]), BF16),
        ),
        scratch_shapes=[
            pltpu.VMEM((rows, width), BF16),
            pltpu.VMEM((1, width), F32),
            pltpu.VMEM((heads, width), BF16),
            pltpu.VMEM((part, widths[2]), BF16),
            pltpu.SemaphoreType.DMA((3,)),
            pltpu.SemaphoreType.DMA((9,)),
        ],
        name="prep",
    )(inputs, gain.reshape(1, -1), w_step_t, *arrays)


def project_kernel(has_rim, x_ref, *rest):
    rim_ref, rest = (rest[0], rest[1:]) if has_rim else (None, rest)
    w_ref, out_hbm = rest[:2]
    kept, (out_ref, sems) = rest[2:-2], rest[-2:]
    width = out_hbm.shape[2]
    weights = w_ref[:, 0:width]
    copies = []
    for f in range(4):
        rows = x_ref[f, 0:BLOCK, :]
        if has_rim:
            rows = jnp.concatenate([rim_ref[f], rows], axis=0)
        out_ref[f] = jnp.dot(rows, weights, preferred_element_type=F32)
        copies.append(pltpu.make_async_copy(out_ref.at[f], out_hbm.at[f], sems.at[f]))
        copies[-1].start()
    for ref in kept:
        ref[...] = w_ref[:, width:]
    for copy in copies:
        copy.wait()


def project_call(x, rim, w, width):
    whole = pl.BlockSpec(memory_space=pltpu.VMEM)
    rows = BLOCK if rim is None else ROWS
    outs = [jax.ShapeDtypeStruct((4, rows, width), F32)]
    specs = [pl.BlockSpec(memory_space=pltpu.HBM)]
    if w.shape[1] > width:
        outs.append(jax.ShapeDtypeStruct((w.shape[0], w.shape[1] - width), BF16))
        specs.append(whole)
    given = [x, w] if rim is None else [x, rim, w]
    return pl.pallas_call(
        functools.partial(project_kernel, rim is not None),
        in_specs=[whole] * len(given),
        out_specs=specs,
        out_shape=outs,
        scratch_shapes=[pltpu.VMEM((4, rows, width), F32), pltpu.SemaphoreType.DMA((4,))],
        compiler_params=vmem(),
        name="project",
    )(*given)


def rim_kernel(ids, rim_ref, w_ref, *outs):
    rows = rim_ref[...].reshape(4 * HALO, 512)
    act = jnp.dot(rows, w_ref[:, 512:], preferred_element_type=F32)
    for f in range(4):
        for r in range(4):

            @pl.when((f + 4 - ids[2]) % 4 == r)
            def _(f=f, r=r):
                outs[r][...] = act[f * HALO : (f + 1) * HALO]


def rim_call(ids, rim, w):
    width = w.shape[1] - 512
    full = lambda *shape: pl.BlockSpec(shape, lambda i, ids: (0,) * len(shape))
    return pl.pallas_call(
        rim_kernel,
        grid_spec=pltpu.PrefetchScalarGridSpec(
            num_scalar_prefetch=1,
            grid=(1,),
            in_specs=[full(*rim.shape), full(*w.shape)],
            out_specs=[full(HALO, width)] * 4,
        ),
        out_shape=[jax.ShapeDtypeStruct((HALO, width), F32)] * 4,
        compiler_params=vmem(),
        name="project_rim",
    )(ids, rim, w)


def added(ref, at, width):
    total = ref[0, :, at : at + width].astype(F32)
    for j in range(1, 4):
        total = total + ref[j, :, at : at + width].astype(F32)
    return total.astype(BF16)


def convolved(wide_ref, taps):
    summed = None
    for i in range(CONV):
        at = HALO - CONV + 1 + i
        part = taps[i : i + 1] * wide_ref[at : at + BLOCK, :]
        summed = part if summed is None else summed + part
    return silu(summed).astype(BF16)


def local_kernel(
    ids, rate, act_ref, e0, e1, e2, e3, step_ref, off_ref, ci_ref, cb_ref, buf_ref,
    send_hbm, xin_ref, bkey_ref, rows_ref, cols_ref, wide_ref, send_ref, sems,
):
    tensor = ids[1]
    moved = pull(
        [
            (buf_ref.at[f, pl.ds(BLOCK, HALO)], send_hbm.at[pl.ds(KEPT + HALO * f, HALO)])
            for f in range(4)
        ],
        sems,
    )
    send_ref[0:BLOCK, :] = added(act_ref, 0, 512)
    moved.append(
        pltpu.make_async_copy(
            send_ref.at[pl.ds(0, BLOCK)], send_hbm.at[pl.ds(0, BLOCK)], sems.at[4]
        )
    )
    moved[-1].start()
    edge = e0[...].astype(F32) + e1[...].astype(F32)
    edge = edge + (e2[...].astype(F32) + e3[...].astype(F32))
    wide_ref[0:HALO, :] = edge.astype(BF16).astype(F32)
    wide_ref[HALO:, :] = added(act_ref, 512, 384).astype(F32)
    conv = convolved(wide_ref, jnp.concatenate([ci_ref[...], cb_ref[...]], axis=1))
    xin, bkey = conv[:, 0:256], conv[:, 256:384]
    xin_ref[...] = xin
    bkey_ref[...] = bkey
    row = iota((BLOCK, BLOCK), 0)
    col = iota((BLOCK, BLOCK), 1)
    step = jnp.concatenate([step_ref[pl.ds(4 * tensor + h, 1), :] for h in range(4)], axis=0)
    rates = jnp.concatenate(
        [jnp.full((1, BLOCK), rate[4 * tensor + h], F32) for h in range(4)], axis=0
    )
    decay = off_ref[...] - rates * step
    decay8 = jnp.concatenate([decay, jnp.zeros((4, BLOCK), F32)], axis=0)
    upper = (row <= col).astype(F32)
    cum = jnp.dot(decay8, upper, precision=HIGH, preferred_element_type=F32)
    last = jnp.sum(decay, axis=1, keepdims=True)
    to_end = jnp.exp(last - cum[0:4]) * step
    eye = (row == col).astype(F32)
    cols = lax.dot_general(
        eye, jnp.concatenate([cum[0:4], to_end], axis=0), NT, precision=HIGH,
        preferred_element_type=F32,
    )
    rows_ref[...] = jnp.concatenate([cum[0:4], step], axis=0)
    cols_ref[...] = cols
    wide_key = bkey.astype(F32)
    for h in range(4):
        wk = (wide_key * cols[:, 4 + h : 5 + h]).astype(BF16)
        state = lax.dot_general(
            xin[:, h * 64 : (h + 1) * 64], wk, TN, preferred_element_type=F32
        )
        log = jnp.broadcast_to(last[h : h + 1], (8, BLOCK))
        high = log.astype(BF16).astype(F32)
        logs = jnp.concatenate([high, log - high], axis=0).astype(BF16)
        send_ref[BLOCK : BLOCK + 64, h * 128 : (h + 1) * 128] = state.astype(BF16)
        send_ref[BLOCK + 64 : KEPT, h * 128 : (h + 1) * 128] = logs
    kept = pl.ds(BLOCK, KEPT - BLOCK)
    moved.append(pltpu.make_async_copy(send_ref.at[kept], send_hbm.at[kept], sems.at[5]))
    moved[-1].start()
    for copy in moved:
        copy.wait()


def local_call(ids, rate, act, rim, step, offset, conv_weight, buf):
    full = lambda *shape: pl.BlockSpec(shape, lambda i, ids, rate: (0,) * len(shape))
    return pl.pallas_call(
        local_kernel,
        grid_spec=pltpu.PrefetchScalarGridSpec(
            num_scalar_prefetch=2,
            grid=(1,),
            in_specs=[
                full(*act.shape),
                *(full(*e.shape) for e in rim),
                full(*step.shape),
                full(*offset.shape),
                pl.BlockSpec((CONV, 256), lambda i, ids, rate: (0, ids[1])),
                pl.BlockSpec((CONV, 128), lambda i, ids, rate: (0, 16 + ids[1])),
                pl.BlockSpec(memory_space=pl.ANY),
            ],
            out_specs=[
                pl.BlockSpec(memory_space=pltpu.HBM), full(BLOCK, 256), full(BLOCK, 128),
                full(8, BLOCK),
                full(BLOCK, 8),
            ],
            scratch_shapes=[
                pltpu.VMEM((ROWS, 384), F32),
                pltpu.VMEM((KEPT, 512), BF16),
                pltpu.SemaphoreType.DMA((6,)),
            ],
        ),
        out_shape=(
            jax.ShapeDtypeStruct((SENT, 512), BF16),
            jax.ShapeDtypeStruct((BLOCK, 256), BF16),
            jax.ShapeDtypeStruct((BLOCK, 128), BF16),
            jax.ShapeDtypeStruct((8, BLOCK), F32),
            jax.ShapeDtypeStruct((BLOCK, 8), F32),
        ),
        name="ssd_local",
    )(ids, rate, act, *rim, step, offset, conv_weight, conv_weight, buf)


def inner_kernel(
    ids, act_ref, cc_ref, xin_ref, bkey_ref, rows_ref, cols_ref,
    yin_ref, gate_ref, cq_ref, q_ref, wide_ref,
):
    gate_ref[...] = silu(added(act_ref, 0, 256)[HALO:].astype(F32))
    q_ref[...] = added(act_ref, 384, 256)[HALO:]
    wide_ref[...] = added(act_ref, 256, 128).astype(F32)
    cquery = convolved(wide_ref, cc_ref[...])
    cq_ref[...] = cquery
    lower = iota((BLOCK, BLOCK), 0) >= iota((BLOCK, BLOCK), 1)
    inner = lax.dot_general(cquery, bkey_ref[...], NT, preferred_element_type=F32)
    for h in range(4):
        spread = cols_ref[:, h : h + 1] - rows_ref[h : h + 1, :]
        decayed = jnp.exp(jnp.where(lower, spread, 0.0))
        mix = jnp.where(lower, inner * decayed * rows_ref[4 + h : 5 + h, :], 0.0).astype(BF16)
        yin_ref[:, h * 64 : (h + 1) * 64] = jnp.dot(
            mix, xin_ref[:, h * 64 : (h + 1) * 64], preferred_element_type=F32
        )


def inner_call(ids, act, conv_weight, xin, bkey, rows, cols):
    full = lambda *shape: pl.BlockSpec(shape, lambda i, ids: (0,) * len(shape))
    return pl.pallas_call(
        inner_kernel,
        grid_spec=pltpu.PrefetchScalarGridSpec(
            num_scalar_prefetch=1,
            grid=(1,),
            in_specs=[
                full(*act.shape),
                pl.BlockSpec((CONV, 128), lambda i, ids: (0, 24 + ids[1])),
                full(BLOCK, 256), full(BLOCK, 128), full(8, BLOCK), full(BLOCK, 8),
            ],
            out_specs=[full(BLOCK, 256), full(BLOCK, 256), full(BLOCK, 128), full(BLOCK, 256)],
            scratch_shapes=[pltpu.VMEM((BLOCK + HALO, 128), F32)],
        ),
        out_shape=(
            jax.ShapeDtypeStruct((BLOCK, 256), F32),
            jax.ShapeDtypeStruct((BLOCK, 256), F32),
            jax.ShapeDtypeStruct((BLOCK, 128), BF16),
            jax.ShapeDtypeStruct((BLOCK, 256), BF16),
        ),
        compiler_params=vmem(),
        name="ssd_inner",
    )(ids, act, conv_weight, xin, bkey, rows, cols)


KEYS = 512
KEPT = BLOCK + 80
SENT = KEPT + 64
LOG2E = 1.4426950408889634


def attend_kernel(
    ids, bias, q_ref, yin_ref, gate_ref, cq_ref, cols_ref, gain_ref, all_hbm, a0, a1, a2, a3,
    out_ref, kv_ref, st_ref, wm_ref, wa_ref, acc_ref, late_ref, hold_ref, sems, ksems, gsems,
):
    block, tensor, mine = ids[0], ids[1], ids[2]
    per = KEYS // BLOCK
    count = all_hbm.shape[0]
    chunks = range(count // per - 1, -1, -1)
    last = block // per

    def move(chunk):
        picked = pl.ds(chunk * per, per)
        return pltpu.make_async_copy(
            all_hbm.at[picked, pl.ds(0, BLOCK)], kv_ref.at[picked], ksems.at[chunk]
        )

    def states(group):
        picked = pl.ds(group * per, per)
        return pltpu.make_async_copy(
            all_hbm.at[picked, pl.ds(BLOCK, 80)], st_ref.at[picked], gsems.at[group]
        )

    weights = [pltpu.make_async_copy(all_hbm.at[:, pl.ds(KEPT, 64)], wm_ref, sems.at[0])]
    weights += [
        pltpu.make_async_copy(w, wa_ref.at[(mine + 4 - r) % 4], sems.at[1 + r])
        for r, w in enumerate((a0, a1, a2, a3))
    ]
    for group in range(count // per):
        pl.when(group * per < block)(lambda group=group: states(group).start())
    for chunk in chunks:
        pl.when((chunk <= last) & (chunk >= last - 1))(lambda chunk=chunk: move(chunk).start())
    acc_ref[...] = jnp.zeros_like(acc_ref)
    late_ref[...] = jnp.zeros_like(late_ref)
    hold_ref[...] = jnp.zeros_like(hold_ref)
    for group in range(count // per):
        pl.when(group * per < block)(lambda group=group: states(group).wait())

    def advance(k, carry):
        logs = st_ref[k, 64:80, :].astype(F32)
        decay = jnp.exp(logs[0:8] + logs[8:16])
        hold_ref[...] = hold_ref[...] * jnp.concatenate([decay] * 8, axis=0) + st_ref[
            k, 0:64, :
        ].astype(F32)
        return carry

    lax.fori_loop(0, block, advance, 0)
    cquery = cq_ref[...]
    ys = []
    for h in range(4):
        enter = hold_ref[:, h * 128 : (h + 1) * 128].astype(BF16)
        moved = lax.dot_general(cquery, enter, NT, preferred_element_type=F32)
        ys.append(moved * jnp.exp(cols_ref[:, h : h + 1]))
    gated = (yin_ref[...] + jnp.concatenate(ys, axis=1)) * gate_ref[...]
    scale = lax.rsqrt(jnp.mean(gated * gated, axis=-1, keepdims=True) + EPS)
    mixed = (gated * scale * gain_ref[...]).astype(BF16)
    row = iota((256, 256), 0) % 128
    col = iota((256, 256), 1)
    onward = ((row > col) | (col >= 128)).astype(BF16)

    def piece(turn, carry):
        chunk = last - turn
        move(chunk).wait()
        pl.when(chunk > 1)(lambda: move(chunk - 2).start())

        @pl.when(turn == jnp.minimum(last, 1))
        def _():
            for copy in weights:
                copy.start()

        picked = pl.ds(chunk * per, per)
        before = [
            chunk * KEYS + sub * BLOCK + iota((BLOCK, BLOCK), 1)
            < block * BLOCK + iota((BLOCK, BLOCK), 0)
            for sub in range(per)
        ]
        taken, parts = {}, []
        for h in range(2):
            query = q_ref[:, h * 128 : (h + 1) * 128]
            key = kv_ref[picked, :, h * 128 : (h + 1) * 128].reshape(KEYS, 128)
            logits = lax.dot_general(query, key, NT, preferred_element_type=F32)
            logits = logits * (128 ** -0.5 * LOG2E) + bias[2 * tensor + h] * LOG2E
            soft = jnp.maximum(logits, 0.0) + LOG2E * jnp.log(1.0 + jnp.exp2(-jnp.abs(logits)))
            for sub in range(per):
                at = slice(sub * BLOCK, (sub + 1) * BLOCK)
                taken[h, sub] = logits[:, at] - soft[:, at]
                kept = jnp.where(before[sub], soft[:, at], 0.0)
                high = kept.astype(BF16)
                low = (kept - high.astype(F32)).astype(BF16)
                parts.append(jnp.concatenate([high, low], axis=1))
        sums = jnp.dot(jnp.concatenate(parts, axis=0), onward, preferred_element_type=F32)
        for h in range(2):
            late = late_ref[h]
            weights_h = [None] * per
            for sub in range(per - 1, -1, -1):
                at = (h * per + sub) * BLOCK
                mine_sums = sums[at : at + BLOCK]
                weight = jnp.exp2(taken[h, sub] - (mine_sums[:, 0:128] + late))
                weights_h[sub] = jnp.where(before[sub], weight, 0.0).astype(BF16)
                late = late + mine_sums[:, 128:256]
            value = kv_ref[picked, :, 256 + h * 128 : 256 + (h + 1) * 128].reshape(KEYS, 128)
            acc_ref[h] += jnp.dot(
                jnp.concatenate(weights_h, axis=1), value, preferred_element_type=F32
            )
            late_ref[h] = late
        return carry

    lax.fori_loop(0, last + 1, piece, 0)
    attended = jnp.concatenate([acc_ref[0].astype(BF16), acc_ref[1].astype(BF16)], axis=1)
    for copy in weights:
        copy.wait()
    for s in range(count):
        halves = []
        for f in range(4):
            for half in range(2):
                halves.append(
                    wm_ref[s, 16 * f : 16 * (f + 1), 256 * half : 256 * (half + 1)]
                )
        rows_m = jnp.concatenate(halves, axis=0)
        rows_a = jnp.concatenate(
            [wa_ref[f, 32 * s : 32 * (s + 1), :] for f in range(4)], axis=0
        )
        out_ref[:, 128 * s : 128 * (s + 1)] = (
            lax.dot_general(mixed, rows_m, NT, preferred_element_type=F32)
            + lax.dot_general(attended, rows_a, NT, preferred_element_type=F32)
        ).astype(BF16)


def attend_call(ids, bias, q, yin, gate, cq, cols, gain, gathered, rows):
    full = lambda *shape: pl.BlockSpec(shape, lambda i, ids, bias: (0,) * len(shape))
    count = gathered.shape[0]
    near = pl.BlockSpec(memory_space=pltpu.VMEM)
    return pl.pallas_call(
        attend_kernel,
        grid_spec=pltpu.PrefetchScalarGridSpec(
            num_scalar_prefetch=2,
            grid=(1,),
            in_specs=[
                full(BLOCK, 256), full(BLOCK, 256), full(BLOCK, 256), full(BLOCK, 128),
                full(BLOCK, 8), pl.BlockSpec((1, 256), lambda i, ids, bias: (0, ids[1])),
                pl.BlockSpec(memory_space=pltpu.HBM), near, near, near, near,
            ],
            out_specs=full(BLOCK, 2048),
            scratch_shapes=[
                pltpu.VMEM((count, BLOCK, 512), BF16),
                pltpu.VMEM((count, 80, 512), BF16),
                pltpu.VMEM((count, 64, 512), BF16),
                pltpu.VMEM((4, 512, 256), BF16),
                pltpu.VMEM((2, BLOCK, 128), F32),
                pltpu.VMEM((2, BLOCK, 128), F32),
                pltpu.VMEM((64, 512), F32),
                pltpu.SemaphoreType.DMA((5,)),
                pltpu.SemaphoreType.DMA((count * BLOCK // KEYS,)),
                pltpu.SemaphoreType.DMA((count * BLOCK // KEYS,)),
            ],
        ),
        out_shape=jax.ShapeDtypeStruct((BLOCK, 2048), BF16),
        compiler_params=vmem(),
        name="attend",
    )(ids, bias, q, yin, gate, cq, cols, gain.reshape(1, -1), gathered, *rows)


def rotated(shard, axis, by):
    length = lax.axis_size(axis)
    return lax.ppermute(shard, axis, [(i, (i + by) % length) for i in range(length)])


def body(
    inputs, norm_gain, w_gate, w_input, w_bkey, w_cquery, w_step, conv_weight, decay_rate,
    decay_offset, ssd_gain, w_query, w_key, w_value, stick_bias, out_mixer, out_attend,
):
    length = lax.axis_size("sp")
    ids = jnp.stack([lax.axis_index(name) for name in ("sp", "tp", "fs")]).astype(jnp.int32)
    split, step, first, second = prep_call(
        inputs, norm_gain, w_step.T, w_key, w_value, w_input, w_bkey, w_gate, w_cquery, w_query,
        out_attend.T, out_mixer.T,
    )
    tokens = lax.all_to_all(split, "fs", 0, 0, tiled=True)
    early = lax.all_gather(first, "sp", axis=0, tiled=True)
    tokens, early = lax.optimization_barrier((tokens, early))
    rim = lax.ppermute(
        tokens[:, BLOCK - HALO : BLOCK], "sp", [(i, i + 1) for i in range(length - 1)]
    )

    def back(act):
        return lax.all_to_all(act, "fs", 0, 0, tiled=True)

    (act,) = project_call(tokens, None, early, 896)
    act = back(act)
    edge = rim_call(ids, rim, early)
    edge = [edge[0]] + [rotated(edge[by], "fs", by) for by in (1, 2, 3)]
    send, xin, bkey, srows, scols = local_call(
        ids, decay_rate, act, edge, step, decay_offset[0].T, conv_weight, tokens
    )
    gathered = lax.all_gather(send, "sp", axis=0)
    act, kept = project_call(tokens, rim, lax.all_gather(second, "sp", axis=0, tiled=True), 640)
    act = back(act)
    rows = [kept] + [rotated(kept, "fs", by) for by in (1, 2, 3)]
    yin, gate, cq, q = inner_call(ids, act, conv_weight, xin, bkey, srows, scols)
    partial = attend_call(ids, stick_bias, q, yin, gate, cq, scols, ssd_gain, gathered, rows)
    parts = lax.all_to_all(partial.reshape(8, 16, 2048), "tp", 0, 0, tiled=True)
    return jnp.sum(parts.astype(F32), axis=0).astype(BF16)[None]


def solution(mesh):
    shard = P(("sp", "fs"), "tp")
    return jax.shard_map(
        body,
        mesh=mesh,
        in_specs=(
            P("fs", "sp", None), P(), shard, shard, shard, shard, P(), P(), P(),
            P("fs", "sp", "tp"), P(), shard, shard, shard, P(),
            P("tp", ("sp", "fs")), P("tp", ("sp", "fs")),
        ),
        out_specs=P("fs", ("sp", "tp"), None),
        check_vma=False,
    )
```

profile of v0, /device:TPU:1, one launch (start us, length us, event | category | flops | bytes accessed | tf_op | source)
XLA Modules:
  0.0 193.1 jit_solution(13189300771370315462)
XLA Ops:
  6.5 2.9 %prep.1 = (bf16[4,144,512]{2,1,0:T(8,128)(2,1)}, f32[32,128]{1,0:T(8,128)}, bf16[32,896]{1,0:T(8,128)(2,1)}, bf16[32,896]{1,0:T(8,128)(2,1)}) custom-call(bf16[1,128,2048]{2,1,0:T(8,128)(2,1)} %refs_0_.1, f32[1,2048]{1,0:T(1,128)} %bitcast.20, bf16[32,2048]{1,0:T(8,128)(2,1)} %bitcast.17, bf16[32,256]{1,0:T(8,128)(2,1)} %refs_3_.1, bf16[32,256]{1,0:T(8,128)(2,1)} %refs_4_.1, ...), custom_call_target="tpu_custom_call" | custom-call | tf_op jit(solution)/shard_map/prep/pallas_call | solution.py:103
  9.4 5.0 %all-to-all-start = ((bf16[4,144,512]{2,1,0:T(8,128)(2,1)}), bf16[4,144,512]{2,1,0:T(8,128)(2,1)S(1)}, u32[]{:S(2)}, u32[]{:S(2)}) async-start(bf16[4,144,512]{2,1,0:T(8,128)(2,1)} %get-tuple-element.26), calls=%async_computation | async-start | bytes 1179648 | tf_op jit(solution)/shard_map/all_to_all | solution.py:538
  14.4 34.2 %all_gather.12.rest_0_.w_ref = bf16[512,896]{1,0:T(8,128)(2,1)S(1)} all-gather(bf16[32,896]{1,0:T(8,128)(2,1)} %get-tuple-element.27), channel_id=1, replica_groups=mesh['sp'=16,'fs'=4,'tp'=8] {'sp'}, dimensions={0}, use_global_device_ids=true | all-gather | bytes 974848 | tf_op jit(solution)/shard_map/all_gather | solution.py:539
  48.7 1.6 project.3
  50.3 4.8 %all-to-all-start.2 = ((f32[4,128,896]{2,1,0:T(8,128)}), f32[4,128,896]{2,1,0:T(8,128)}, u32[]{:S(2)}, u32[]{:S(2)}) async-start(f32[4,128,896]{2,1,0:T(8,128)} %project.3), calls=%async_computation.2 | async-start | bytes 3670016 | tf_op jit(solution)/shard_map/all_to_all | solution.py:546
  55.0 1.5 collective-permute-start
  56.5 0.1 pad_add_fusion.ids
  56.6 1.2 collective-permute-done.rest_0_.rim_ref
  57.8 0.9 project_rim.1
  58.8 0.6 copy-done.6
  59.3 3.5 %collective-permute-start.1 = (f32[16,384]{1,0:T(8,128)S(1)}, f32[16,384]{1,0:T(8,128)S(1)}, u32[]{:S(2)}, u32[]{:S(2)}) collective-permute-start(f32[16,384]{1,0:T(8,128)S(1)} %get-tuple-element.33), channel_id=1, source_target_pairs={{0,8},{8,16},{16,24},{24,0},{1,9},{9,17},{17,25},{25,1},{2,10},{10... | collective-permute-start | bytes 73736 | tf_op jit(solution)/shard_map/ppermute | solution.py:525
  62.8 4.5 %collective-permute-start.2 = (f32[16,384]{1,0:T(8,128)S(1)}, f32[16,384]{1,0:T(8,128)S(1)}, u32[]{:S(2)}, u32[]{:S(2)}) collective-permute-start(f32[16,384]{1,0:T(8,128)S(1)} %get-tuple-element.34), channel_id=1, source_target_pairs={{0,16},{8,24},{16,0},{24,8},{1,17},{9,25},{17,1},{25,9},{2,18},{10... | collective-permute-start | bytes 73736 | tf_op jit(solution)/shard_map/ppermute | solution.py:525
  67.4 3.0 %collective-permute-start.3 = (f32[16,384]{1,0:T(8,128)S(1)}, f32[16,384]{1,0:T(8,128)S(1)}, u32[]{:S(2)}, u32[]{:S(2)}) collective-permute-start(f32[16,384]{1,0:T(8,128)S(1)} %get-tuple-element.35), channel_id=1, source_target_pairs={{0,24},{8,0},{16,8},{24,16},{1,25},{9,1},{17,9},{25,17},{2,26},{10... | collective-permute-start | bytes 73736 | tf_op jit(solution)/shard_map/ppermute | solution.py:525
  70.3 1.0 collective-permute-done.2.e2
  71.4 1.2 collective-permute-done.3.e3
  72.6 0.6 copy-done.15
  73.2 6.2 %ssd_local.1 = (bf16[272,512]{1,0:T(8,128)(2,1)}, bf16[128,256]{1,0:T(8,128)(2,1)}, bf16[128,128]{1,0:T(8,128)(2,1)}, f32[8,128]{1,0:T(8,128)}, f32[128,8]{1,0:T(8,128)}) custom-call(s32[3]{0:T(128)} %copy-done.7, f32[32]{0:T(128)} %rate.1, f32[4,128,896]{2,1,0:T(8,128)} %all-to-all-done.2.act_ref, f32[16,384]{1,0:T(8,128)} %copy-done.6, ...), custom_call_target="tpu_custom_call" | custom-call | tf_op jit(solution)/shard_map/ssd_local/pallas_call | solution.py:274
  79.4 0.0 all-gather.3.cloned.1.call-update
  79.4 28.2 %all_gather.13.rest_1_ = bf16[512,896]{1,0:T(8,128)(2,1)S(1)} all-gather(bf16[32,896]{1,0:T(8,128)(2,1)S(1)} %copy-done.12), channel_id=1, replica_groups=mesh['sp'=16,'fs'=4,'tp'=8] {'sp'}, dimensions={0}, use_global_device_ids=true | all-gather | bytes 974848 | tf_op jit(solution)/shard_map/all_gather | solution.py:556
  107.6 1.5 project.2
  109.2 4.5 %all-to-all-start.1 = ((f32[4,144,640]{2,1,0:T(8,128)}), f32[4,144,640]{2,1,0:T(8,128)S(1)}, u32[]{:S(2)}, u32[]{:S(2)}) async-start(f32[4,144,640]{2,1,0:T(8,128)} %get-tuple-element.30), calls=%async_computation.1 | async-start | bytes 2949120 | tf_op jit(solution)/shard_map/all_to_all | solution.py:546
  113.7 3.4 %collective-permute-start.4 = (bf16[512,256]{1,0:T(8,128)(2,1)S(1)}, bf16[512,256]{1,0:T(8,128)(2,1)S(1)}, u32[]{:S(2)}, u32[]{:S(2)}) collective-permute-start(bf16[512,256]{1,0:T(8,128)(2,1)S(1)} %get-tuple-element.46.a0), channel_id=1, source_target_pairs={{0,8},{8,16},{16,24},{24,0},{1,9},{9,17},{17,25},{25,1},{2,10},{10... | collective-permute-start | bytes 786440 | tf_op jit(solution)/shard_map/ppermute | solution.py:525
  117.1 4.3 %collective-permute-start.5 = (bf16[512,256]{1,0:T(8,128)(2,1)S(1)}, bf16[512,256]{1,0:T(8,128)(2,1)S(1)}, u32[]{:S(2)}, u32[]{:S(2)}) collective-permute-start(bf16[512,256]{1,0:T(8,128)(2,1)S(1)} %get-tuple-element.46.a0), channel_id=1, source_target_pairs={{0,16},{8,24},{16,0},{24,8},{1,17},{9,25},{17,1},{25,9},{2,18},{10... | collective-permute-start | bytes 786440 | tf_op jit(solution)/shard_map/ppermute | solution.py:525
  121.4 3.1 %collective-permute-start.6 = (bf16[512,256]{1,0:T(8,128)(2,1)S(1)}, bf16[512,256]{1,0:T(8,128)(2,1)S(1)}, u32[]{:S(2)}, u32[]{:S(2)}) collective-permute-start(bf16[512,256]{1,0:T(8,128)(2,1)S(1)} %get-tuple-element.46.a0), channel_id=1, source_target_pairs={{0,24},{8,0},{16,8},{24,16},{1,25},{9,1},{17,9},{25,17},{2,26},{10... | collective-permute-start | bytes 786440 | tf_op jit(solution)/shard_map/ppermute | solution.py:525
  124.5 1.4 all-to-all-done.1.act_ref
  125.9 1.0 ssd_inner.1
  126.9 1.7 collective-permute-done.4.a1
  128.6 2.7 %collective-permute-done.5.a2 = bf16[512,256]{1,0:T(8,128)(2,1)S(1)} collective-permute-done((bf16[512,256]{1,0:T(8,128)(2,1)S(1)}, bf16[512,256]{1,0:T(8,128)(2,1)S(1)}, u32[]{:S(2)}, u32[]{:S(2)}) %collective-permute-start.5) | collective-permute-done | bytes 262176 | tf_op jit(solution)/shard_map/ppermute | solution.py:525
  131.4 29.0 %all-gather.3.cloned.1.call-done = bf16[4352,512]{1,0:T(8,128)(2,1)} async-done(((bf16[272,512]{1,0:T(8,128)(2,1)}), bf16[4352,512]{1,0:T(8,128)(2,1)}) %all-gather.3.cloned.1.call-update) | async-done | bytes 4456464 | tf_op jit(solution)/shard_map/all_gather | solution.py:555
  160.4 3.7 %attend.1 = bf16[128,2048]{1,0:T(8,128)(2,1)S(1)} custom-call(s32[3]{0:T(128)S(1)} %copy-done.8, f32[16]{0:T(128)S(1)} %copy-done.11, bf16[128,256]{1,0:T(8,128)(2,1)S(1)} %get-tuple-element.41.q_ref, f32[128,256]{1,0:T(8,128)S(1)} %get-tuple-element.42.yin_ref, f32[128,256]{1,0:T(8,128)S(1)} %get-tuple-element.43.gate_ref, ...), custom_call_target="tpu_custom_call" | custom-call | tf_op jit(solution)/shard_map/attend/pallas_call | solution.py:493
  164.1 21.5 %all_to_all.20 = bf16[8,16,2048]{2,1,0:T(8,128)(2,1)S(1)} all-to-all(bf16[8,16,2048]{2,1,0:T(8,128)(2,1)S(1)} %bitcast.14), channel_id=1, replica_groups=mesh['sp'=16,'fs'=4,'tp'=8] {'tp'}, dimensions={0} | all-to-all | bytes 1048576 | tf_op jit(solution)/shard_map/all_to_all | solution.py:561
  185.6 0.7 reduce_sum.12
  (36 shorter events, 0.1 us)
Async XLA Ops:
  9.4 39.2 %all-to-all-start = ((bf16[4,144,512]{2,1,0:T(8,128)(2,1)}), bf16[4,144,512]{2,1,0:T(8,128)(2,1)S(1)}, u32[]{:S(2)}, u32[]{:S(2)}) async-start(bf16[4,144,512]{2,1,0:T(8,128)(2,1)} %get-tuple-element.26), calls=%async_computation | async-start | bytes 1179648 | tf_op jit(solution)/shard_map/all_to_all | solution.py:538
  48.7 6.4 %copy-start = (bf16[4,144,512]{2,1,0:T(8,128)(2,1)}, bf16[4,144,512]{2,1,0:T(8,128)(2,1)S(1)}, u32[]{:S(2)}) copy-start(bf16[4,144,512]{2,1,0:T(8,128)(2,1)S(1)} %all-to-all-done.x_ref.buf_ref) | copy-start | bytes 1769476
  50.3 22.3 %all-to-all-start.2 = ((f32[4,128,896]{2,1,0:T(8,128)}), f32[4,128,896]{2,1,0:T(8,128)}, u32[]{:S(2)}, u32[]{:S(2)}) async-start(f32[4,128,896]{2,1,0:T(8,128)} %project.3), calls=%async_computation.2 | async-start | bytes 3670016 | tf_op jit(solution)/shard_map/all_to_all | solution.py:546
  55.0 105.4 %all-gather.3.cloned.1.call-start = ((), (), s32[]{:S(2)}) async-start(), calls=%async_computation.4 | async-start | bytes 4734976 | tf_op jit(solution)/shard_map/all_gather | solution.py:555
  55.0 2.8 %collective-permute-start = (bf16[4,16,512]{2,1,0:T(8,128)(2,1)S(1)}, bf16[4,16,512]{2,1,0:T(8,128)(2,1)S(1)}, u32[]{:S(2)}, u32[]{:S(2)}) collective-permute-start(bf16[4,16,512]{2,1,0:T(8,128)(2,1)S(1)} %slice.3), channel_id=1, source_target_pairs={{0,32},{32,64},{64,96},{96,128},{128,160},{160,192},{192,224},{224... | collective-permute-start | bytes 196616 | tf_op jit(solution)/shard_map/ppermute | solution.py:541
  56.6 16.0 %copy-start.7 = (s32[3]{0:T(128)}, s32[3]{0:T(128)S(1)}, u32[]{:S(2)}) copy-start(s32[3]{0:T(128)S(1)} %pad_add_fusion.ids) | copy-start | bytes 40
  56.6 22.8 %copy-start.12 = (bf16[32,896]{1,0:T(8,128)(2,1)S(1)}, bf16[32,896]{1,0:T(8,128)(2,1)}, u32[]{:S(2)}) copy-start(bf16[32,896]{1,0:T(8,128)(2,1)} %get-tuple-element.29) | copy-start | bytes 172036
  58.7 0.6 copy-start.6
  59.3 11.0 %collective-permute-start.1 = (f32[16,384]{1,0:T(8,128)S(1)}, f32[16,384]{1,0:T(8,128)S(1)}, u32[]{:S(2)}, u32[]{:S(2)}) collective-permute-start(f32[16,384]{1,0:T(8,128)S(1)} %get-tuple-element.33), channel_id=1, source_target_pairs={{0,8},{8,16},{16,24},{24,0},{1,9},{9,17},{17,25},{25,1},{2,10},{10... | collective-permute-start | bytes 73736 | tf_op jit(solution)/shard_map/ppermute | solution.py:525
  62.8 8.5 %collective-permute-start.2 = (f32[16,384]{1,0:T(8,128)S(1)}, f32[16,384]{1,0:T(8,128)S(1)}, u32[]{:S(2)}, u32[]{:S(2)}) collective-permute-start(f32[16,384]{1,0:T(8,128)S(1)} %get-tuple-element.34), channel_id=1, source_target_pairs={{0,16},{8,24},{16,0},{24,8},{1,17},{9,25},{17,1},{25,9},{2,18},{10... | collective-permute-start | bytes 73736 | tf_op jit(solution)/shard_map/ppermute | solution.py:525
  67.4 5.2 %collective-permute-start.3 = (f32[16,384]{1,0:T(8,128)S(1)}, f32[16,384]{1,0:T(8,128)S(1)}, u32[]{:S(2)}, u32[]{:S(2)}) collective-permute-start(f32[16,384]{1,0:T(8,128)S(1)} %get-tuple-element.35), channel_id=1, source_target_pairs={{0,24},{8,0},{16,8},{24,16},{1,25},{9,1},{17,9},{25,17},{2,26},{10... | collective-permute-start | bytes 73736 | tf_op jit(solution)/shard_map/ppermute | solution.py:525
  70.3 2.3 %copy-start.13 = (f32[16,384]{1,0:T(8,128)}, f32[16,384]{1,0:T(8,128)S(1)}, u32[]{:S(2)}) copy-start(f32[16,384]{1,0:T(8,128)S(1)} %collective-permute-done.1.e1) | copy-start | bytes 73732
  71.4 1.3 copy-start.14
  72.6 0.6 copy-start.15
  73.2 34.4 %copy-start.1 = (bf16[4,144,512]{2,1,0:T(8,128)(2,1)S(1)}, bf16[4,144,512]{2,1,0:T(8,128)(2,1)}, u32[]{:S(2)}) copy-start(bf16[4,144,512]{2,1,0:T(8,128)(2,1)} %copy-done) | copy-start | bytes 1769476
  109.1 16.8 %copy-start.2 = (f32[4,4096]{1,0:T(4,128)S(1)}, f32[4,4096]{1,0:T(4,128)}, u32[]{:S(2)}) copy-start(f32[4,4096]{1,0:T(4,128)} %cc_ref.1) | copy-start | bytes 196612
  109.1 16.8 %copy-start.3 = (f32[128,8]{1,0:T(8,128)S(1)}, f32[128,8]{1,0:T(8,128)}, u32[]{:S(2)}) copy-start(f32[128,8]{1,0:T(8,128)} %get-tuple-element.40.cols_ref) | copy-start | bytes 12292
  109.1 16.7 %copy-start.4 = (bf16[128,256]{1,0:T(8,128)(2,1)S(1)}, bf16[128,256]{1,0:T(8,128)(2,1)}, u32[]{:S(2)}) copy-start(bf16[128,256]{1,0:T(8,128)(2,1)} %get-tuple-element.37.xin_ref) | copy-start | bytes 196612
  109.1 16.7 %copy-start.5 = (bf16[128,128]{1,0:T(8,128)(2,1)S(1)}, bf16[128,128]{1,0:T(8,128)(2,1)}, u32[]{:S(2)}) copy-start(bf16[128,128]{1,0:T(8,128)(2,1)} %get-tuple-element.38.bkey_ref) | copy-start | bytes 98308
  109.1 16.7 %copy-start.8 = (s32[3]{0:T(128)S(1)}, s32[3]{0:T(128)}, u32[]{:S(2)}) copy-start(s32[3]{0:T(128)} %copy-done.7) | copy-start | bytes 40
  109.1 16.7 %copy-start.10 = (f32[8,128]{1,0:T(8,128)S(1)}, f32[8,128]{1,0:T(8,128)}, u32[]{:S(2)}) copy-start(f32[8,128]{1,0:T(8,128)} %get-tuple-element.39.rows_ref) | copy-start | bytes 12292
  109.1 51.3 %copy-start.9 = (f32[2048]{0:T(1024)S(1)}, f32[2048]{0:T(1024)}, u32[]{:S(2)}) copy-start(f32[2048]{0:T(1024)} %param.27) | copy-start | bytes 24580
  109.1 51.3 %copy-start.11 = (f32[16]{0:T(128)S(1)}, f32[16]{0:T(128)}, u32[]{:S(2)}) copy-start(f32[16]{0:T(128)} %bias.1) | copy-start | bytes 196
  109.2 16.7 %all-to-all-start.1 = ((f32[4,144,640]{2,1,0:T(8,128)}), f32[4,144,640]{2,1,0:T(8,128)S(1)}, u32[]{:S(2)}, u32[]{:S(2)}) async-start(f32[4,144,640]{2,1,0:T(8,128)} %get-tuple-element.30), calls=%async_computation.1 | async-start | bytes 2949120 | tf_op jit(solution)/shard_map/all_to_all | solution.py:546
  113.7 14.9 %collective-permute-start.4 = (bf16[512,256]{1,0:T(8,128)(2,1)S(1)}, bf16[512,256]{1,0:T(8,128)(2,1)S(1)}, u32[]{:S(2)}, u32[]{:S(2)}) collective-permute-start(bf16[512,256]{1,0:T(8,128)(2,1)S(1)} %get-tuple-element.46.a0), channel_id=1, source_target_pairs={{0,8},{8,16},{16,24},{24,0},{1,9},{9,17},{17,25},{25,1},{2,10},{10... | collective-permute-start | bytes 786440 | tf_op jit(solution)/shard_map/ppermute | solution.py:525
  117.1 14.3 %collective-permute-start.5 = (bf16[512,256]{1,0:T(8,128)(2,1)S(1)}, bf16[512,256]{1,0:T(8,128)(2,1)S(1)}, u32[]{:S(2)}, u32[]{:S(2)}) collective-permute-start(bf16[512,256]{1,0:T(8,128)(2,1)S(1)} %get-tuple-element.46.a0), channel_id=1, source_target_pairs={{0,16},{8,24},{16,0},{24,8},{1,17},{9,25},{17,1},{25,9},{2,18},{10... | collective-permute-start | bytes 786440 | tf_op jit(solution)/shard_map/ppermute | solution.py:525
  121.4 10.0 %collective-permute-start.6 = (bf16[512,256]{1,0:T(8,128)(2,1)S(1)}, bf16[512,256]{1,0:T(8,128)(2,1)S(1)}, u32[]{:S(2)}, u32[]{:S(2)}) collective-permute-start(bf16[512,256]{1,0:T(8,128)(2,1)S(1)} %get-tuple-element.46.a0), channel_id=1, source_target_pairs={{0,24},{8,0},{16,8},{24,16},{1,25},{9,1},{17,9},{25,17},{2,26},{10... | collective-permute-start | bytes 786440 | tf_op jit(solution)/shard_map/ppermute | solution.py:525
Sparse Core Ops, SparseCore 0:
  79.5 80.8 all-gather.2
where the time goes:
time: 194 us; the launch traced here: 193 us
  blocking collectives  83.9 us (43%)
  waiting for transfers between devices  38.3 us (20%)
  starting transfers between devices  37.5 us (19%)
  Pallas kernels  17.7 us (9%)
  between operations  13.7 us (7%)
    all_gather x1, blocking collectives, body(): early = lax.all_gather(first, 'sp', axis=0, tiled=True)  34.2 us
    all_gather x1, waiting for transfers between devices, body(): gathered = lax.all_gather(send, 'sp', axis=0)  29 us
    all_gather x1, blocking collectives, body(): lax.all_gather(second, 'sp', axis=0, tiled=True)  28.2 us
    ppermute x6, starting transfers between devices, rotated(): lax.ppermute(shard, axis, [(i, (i + by) % length) for i in range(length)])  21.7 us
    all_to_all x1, blocking collectives, body(): parts = lax.all_to_all(partial.reshape(8, 16, 2048), 'tp', 0, 0, tiled=True)  21.5 us
    all_to_all x2, starting transfers between devices, back(): return lax.all_to_all(act, 'fs', 0, 0, tiled=True)  9.3 us
    ppermute x6, waiting for transfers between devices, rotated(): lax.ppermute(shard, axis, [(i, (i + by) % length) for i in range(length)])  6.72 us
    pallas_call x1, Pallas kernels, local_call(): pl.pallas_call(local_kernel, grid_spec=pltpu.PrefetchScalarGridSpec(num_s...  6.18 us
  transfers between devices with their start and end apart: 11, of which 7 were waited for; matrix products, arithmetic and copies ran while one was open for 0% of the time, Pallas kernels for 2%

commit v1 on v0

--- a/solution.py
+++ b/solution.py
@@ -169,7 +169,7 @@
 
             @pl.when((f + 4 - ids[2]) % 4 == r)
             def _(f=f, r=r):
-                outs[r][...] = act[f * HALO : (f + 1) * HALO]
+                outs[r][...] = act[f * HALO + 8 : (f + 1) * HALO]
 
 
 def rim_call(ids, rim, w):
@@ -181,9 +181,9 @@
             num_scalar_prefetch=1,
             grid=(1,),
             in_specs=[full(*rim.shape), full(*w.shape)],
-            out_specs=[full(HALO, width)] * 4,
-        ),
-        out_shape=[jax.ShapeDtypeStruct((HALO, width), F32)] * 4,
+            out_specs=[full(8, width)] * 4,
+        ),
+        out_shape=[jax.ShapeDtypeStruct((8, width), F32)] * 4,
         compiler_params=vmem(),
         name="project_rim",
     )(ids, rim, w)
@@ -226,7 +226,7 @@
     moved[-1].start()
     edge = e0[...].astype(F32) + e1[...].astype(F32)
     edge = edge + (e2[...].astype(F32) + e3[...].astype(F32))
-    wide_ref[0:HALO, :] = edge.astype(BF16).astype(F32)
+    wide_ref[8:HALO, :] = edge.astype(BF16).astype(F32)
     wide_ref[HALO:, :] = added(act_ref, 512, 384).astype(F32)
     conv = convolved(wide_ref, jnp.concatenate([ci_ref[...], cb_ref[...]], axis=1))
     xin, bkey = conv[:, 0:256], conv[:, 256:384]

time: 194 us -> 194 us (level)
  no operation moved by 1% of the time
where the time goes in v1:
time: 194 us; the launch traced here: 193 us
  blocking collectives  83.8 us (43%)
  waiting for transfers between devices  38.3 us (20%)
  starting transfers between devices  37.6 us (19%)
  Pallas kernels  17.7 us (9%)
  between operations  13.7 us (7%)
    all_gather x1, blocking collectives, body(): early = lax.all_gather(first, 'sp', axis=0, tiled=True)  34.2 us
    all_gather x1, waiting for transfers between devices, body(): gathered = lax.all_gather(send, 'sp', axis=0)  29.2 us
    all_gather x1, blocking collectives, body(): lax.all_gather(second, 'sp', axis=0, tiled=True)  28.1 us
    ppermute x6, starting transfers between devices, rotated(): lax.ppermute(shard, axis, [(i, (i + by) % length) for i in range(length)])  21.7 us
    all_to_all x1, blocking collectives, body(): parts = lax.all_to_all(partial.reshape(8, 16, 2048), 'tp', 0, 0, tiled=True)  21.4 us
    all_to_all x2, starting transfers between devices, back(): return lax.all_to_all(act, 'fs', 0, 0, tiled=True)  9.36 us
    ppermute x6, waiting for transfers between devices, rotated(): lax.ppermute(shard, axis, [(i, (i + by) % length) for i in range(length)])  6.45 us
    pallas_call x1, Pallas kernels, local_call(): pl.pallas_call(local_kernel, grid_spec=pltpu.PrefetchScalarGridSpec(num_s...  6.18 us
  transfers between devices with their start and end apart: 11, of which 7 were waited for; matrix products, arithmetic and copies ran while one was open for 0% of the time, Pallas kernels for 2%

profile of v1, /device:TPU:1, one launch (start us, length us, event | category | flops | bytes accessed | tf_op | source)
XLA Modules:
  0.0 193.0 jit_solution(10388874349369940187)
XLA Ops:
  6.5 2.9 %prep.1 = (bf16[4,144,512]{2,1,0:T(8,128)(2,1)}, f32[32,128]{1,0:T(8,128)}, bf16[32,896]{1,0:T(8,128)(2,1)}, bf16[32,896]{1,0:T(8,128)(2,1)}) custom-call(bf16[1,128,2048]{2,1,0:T(8,128)(2,1)} %refs_0_.1, f32[1,2048]{1,0:T(1,128)} %bitcast.20, bf16[32,2048]{1,0:T(8,128)(2,1)} %bitcast.17, bf16[32,256]{1,0:T(8,128)(2,1)} %refs_3_.1, bf16[32,256]{1,0:T(8,128)(2,1)} %refs_4_.1, ...), custom_call_target="tpu_custom_call" | custom-call | tf_op jit(solution)/shard_map/prep/pallas_call | solution.py:103
  9.4 5.0 %all-to-all-start = ((bf16[4,144,512]{2,1,0:T(8,128)(2,1)}), bf16[4,144,512]{2,1,0:T(8,128)(2,1)S(1)}, u32[]{:S(2)}, u32[]{:S(2)}) async-start(bf16[4,144,512]{2,1,0:T(8,128)(2,1)} %get-tuple-element.26), calls=%async_computation | async-start | bytes 1179648 | tf_op jit(solution)/shard_map/all_to_all | solution.py:538
  14.4 34.2 %all_gather.12.rest_0_.w_ref = bf16[512,896]{1,0:T(8,128)(2,1)S(1)} all-gather(bf16[32,896]{1,0:T(8,128)(2,1)} %get-tuple-element.27), channel_id=1, replica_groups=mesh['sp'=16,'fs'=4,'tp'=8] {'sp'}, dimensions={0}, use_global_device_ids=true | all-gather | bytes 974848 | tf_op jit(solution)/shard_map/all_gather | solution.py:539
  48.7 1.6 project.3
  50.3 4.8 %all-to-all-start.2 = ((f32[4,128,896]{2,1,0:T(8,128)}), f32[4,128,896]{2,1,0:T(8,128)}, u32[]{:S(2)}, u32[]{:S(2)}) async-start(f32[4,128,896]{2,1,0:T(8,128)} %project.3), calls=%async_computation.2 | async-start | bytes 3670016 | tf_op jit(solution)/shard_map/all_to_all | solution.py:546
  55.0 1.5 collective-permute-start
  56.5 0.1 pad_add_fusion.ids
  56.6 1.2 collective-permute-done.rest_0_.rim_ref
  57.8 0.9 project_rim.1
  58.7 0.6 copy-done.8
  59.3 3.5 %collective-permute-start.1 = (f32[8,384]{1,0:T(8,128)S(1)}, f32[8,384]{1,0:T(8,128)S(1)}, u32[]{:S(2)}, u32[]{:S(2)}) collective-permute-start(f32[8,384]{1,0:T(8,128)S(1)} %get-tuple-element.33), channel_id=1, source_target_pairs={{0,8},{8,16},{16,24},{24,0},{1,9},{9,17},{17,25},{25,1},{2,10},{10... | collective-permute-start | bytes 36872 | tf_op jit(solution)/shard_map/ppermute | solution.py:525
  62.8 4.5 %collective-permute-start.2 = (f32[8,384]{1,0:T(8,128)S(1)}, f32[8,384]{1,0:T(8,128)S(1)}, u32[]{:S(2)}, u32[]{:S(2)}) collective-permute-start(f32[8,384]{1,0:T(8,128)S(1)} %get-tuple-element.34), channel_id=1, source_target_pairs={{0,16},{8,24},{16,0},{24,8},{1,17},{9,25},{17,1},{25,9},{2,18},{10... | collective-permute-start | bytes 36872 | tf_op jit(solution)/shard_map/ppermute | solution.py:525
  67.4 3.0 %collective-permute-start.3 = (f32[8,384]{1,0:T(8,128)S(1)}, f32[8,384]{1,0:T(8,128)S(1)}, u32[]{:S(2)}, u32[]{:S(2)}) collective-permute-start(f32[8,384]{1,0:T(8,128)S(1)} %get-tuple-element.35), channel_id=1, source_target_pairs={{0,24},{8,0},{16,8},{24,16},{1,25},{9,1},{17,9},{25,17},{2,26},{10... | collective-permute-start | bytes 36872 | tf_op jit(solution)/shard_map/ppermute | solution.py:525
  70.3 0.5 collective-permute-done.2.e2
  70.8 1.5 collective-permute-done.3.e3
  72.4 0.6 copy-done.15
  72.9 6.2 %ssd_local.1 = (bf16[272,512]{1,0:T(8,128)(2,1)}, bf16[128,256]{1,0:T(8,128)(2,1)}, bf16[128,128]{1,0:T(8,128)(2,1)}, f32[8,128]{1,0:T(8,128)}, f32[128,8]{1,0:T(8,128)}) custom-call(s32[3]{0:T(128)} %copy-done.6, f32[32]{0:T(128)} %rate.1, f32[4,128,896]{2,1,0:T(8,128)} %all-to-all-done.2.act_ref, f32[8,384]{1,0:T(8,128)} %copy-done.8, ...), custom_call_target="tpu_custom_call" | custom-call | tf_op jit(solution)/shard_map/ssd_local/pallas_call | solution.py:274
  79.1 0.0 all-gather.3.cloned.1.call-update
  79.1 28.1 %all_gather.13.rest_1_ = bf16[512,896]{1,0:T(8,128)(2,1)S(1)} all-gather(bf16[32,896]{1,0:T(8,128)(2,1)S(1)} %copy-done.12), channel_id=1, replica_groups=mesh['sp'=16,'fs'=4,'tp'=8] {'sp'}, dimensions={0}, use_global_device_ids=true | all-gather | bytes 974848 | tf_op jit(solution)/shard_map/all_gather | solution.py:556
  107.3 1.5 project.2
  108.8 4.6 %all-to-all-start.1 = ((f32[4,144,640]{2,1,0:T(8,128)}), f32[4,144,640]{2,1,0:T(8,128)S(1)}, u32[]{:S(2)}, u32[]{:S(2)}) async-start(f32[4,144,640]{2,1,0:T(8,128)} %get-tuple-element.30), calls=%async_computation.1 | async-start | bytes 2949120 | tf_op jit(solution)/shard_map/all_to_all | solution.py:546
  113.4 3.4 %collective-permute-start.4 = (bf16[512,256]{1,0:T(8,128)(2,1)S(1)}, bf16[512,256]{1,0:T(8,128)(2,1)S(1)}, u32[]{:S(2)}, u32[]{:S(2)}) collective-permute-start(bf16[512,256]{1,0:T(8,128)(2,1)S(1)} %get-tuple-element.46.a0), channel_id=1, source_target_pairs={{0,8},{8,16},{16,24},{24,0},{1,9},{9,17},{17,25},{25,1},{2,10},{10... | collective-permute-start | bytes 786440 | tf_op jit(solution)/shard_map/ppermute | solution.py:525
  116.8 4.3 %collective-permute-start.5 = (bf16[512,256]{1,0:T(8,128)(2,1)S(1)}, bf16[512,256]{1,0:T(8,128)(2,1)S(1)}, u32[]{:S(2)}, u32[]{:S(2)}) collective-permute-start(bf16[512,256]{1,0:T(8,128)(2,1)S(1)} %get-tuple-element.46.a0), channel_id=1, source_target_pairs={{0,16},{8,24},{16,0},{24,8},{1,17},{9,25},{17,1},{25,9},{2,18},{10... | collective-permute-start | bytes 786440 | tf_op jit(solution)/shard_map/ppermute | solution.py:525
  121.1 3.1 %collective-permute-start.6 = (bf16[512,256]{1,0:T(8,128)(2,1)S(1)}, bf16[512,256]{1,0:T(8,128)(2,1)S(1)}, u32[]{:S(2)}, u32[]{:S(2)}) collective-permute-start(bf16[512,256]{1,0:T(8,128)(2,1)S(1)} %get-tuple-element.46.a0), channel_id=1, source_target_pairs={{0,24},{8,0},{16,8},{24,16},{1,25},{9,1},{17,9},{25,17},{2,26},{10... | collective-permute-start | bytes 786440 | tf_op jit(solution)/shard_map/ppermute | solution.py:525
  124.2 1.4 all-to-all-done.1.act_ref
  125.6 1.0 ssd_inner.1
  126.7 1.7 collective-permute-done.4.a1
  128.4 2.7 %collective-permute-done.5.a2 = bf16[512,256]{1,0:T(8,128)(2,1)S(1)} collective-permute-done((bf16[512,256]{1,0:T(8,128)(2,1)S(1)}, bf16[512,256]{1,0:T(8,128)(2,1)S(1)}, u32[]{:S(2)}, u32[]{:S(2)}) %collective-permute-start.5) | collective-permute-done | bytes 262176 | tf_op jit(solution)/shard_map/ppermute | solution.py:525
  131.1 29.2 %all-gather.3.cloned.1.call-done = bf16[4352,512]{1,0:T(8,128)(2,1)} async-done(((bf16[272,512]{1,0:T(8,128)(2,1)}), bf16[4352,512]{1,0:T(8,128)(2,1)}) %all-gather.3.cloned.1.call-update) | async-done | bytes 4456464 | tf_op jit(solution)/shard_map/all_gather | solution.py:555
  160.4 3.7 %attend.1 = bf16[128,2048]{1,0:T(8,128)(2,1)S(1)} custom-call(s32[3]{0:T(128)S(1)} %copy-done.7, f32[16]{0:T(128)S(1)} %copy-done.11, bf16[128,256]{1,0:T(8,128)(2,1)S(1)} %get-tuple-element.41.q_ref, f32[128,256]{1,0:T(8,128)S(1)} %get-tuple-element.42.yin_ref, f32[128,256]{1,0:T(8,128)S(1)} %get-tuple-element.43.gate_ref, ...), custom_call_target="tpu_custom_call" | custom-call | tf_op jit(solution)/shard_map/attend/pallas_call | solution.py:493
  164.1 21.4 %all_to_all.20 = bf16[8,16,2048]{2,1,0:T(8,128)(2,1)S(1)} all-to-all(bf16[8,16,2048]{2,1,0:T(8,128)(2,1)S(1)} %bitcast.14), channel_id=1, replica_groups=mesh['sp'=16,'fs'=4,'tp'=8] {'tp'}, dimensions={0} | all-to-all | bytes 1048576 | tf_op jit(solution)/shard_map/all_to_all | solution.py:561
  185.5 0.7 reduce_sum.12
  (36 shorter events, 0.1 us)
Async XLA Ops:
  9.4 39.2 %all-to-all-start = ((bf16[4,144,512]{2,1,0:T(8,128)(2,1)}), bf16[4,144,512]{2,1,0:T(8,128)(2,1)S(1)}, u32[]{:S(2)}, u32[]{:S(2)}) async-start(bf16[4,144,512]{2,1,0:T(8,128)(2,1)} %get-tuple-element.26), calls=%async_computation | async-start | bytes 1179648 | tf_op jit(solution)/shard_map/all_to_all | solution.py:538
  48.7 6.4 %copy-start = (bf16[4,144,512]{2,1,0:T(8,128)(2,1)}, bf16[4,144,512]{2,1,0:T(8,128)(2,1)S(1)}, u32[]{:S(2)}) copy-start(bf16[4,144,512]{2,1,0:T(8,128)(2,1)S(1)} %all-to-all-done.x_ref.buf_ref) | copy-start | bytes 1769476
  50.3 22.1 %all-to-all-start.2 = ((f32[4,128,896]{2,1,0:T(8,128)}), f32[4,128,896]{2,1,0:T(8,128)}, u32[]{:S(2)}, u32[]{:S(2)}) async-start(f32[4,128,896]{2,1,0:T(8,128)} %project.3), calls=%async_computation.2 | async-start | bytes 3670016 | tf_op jit(solution)/shard_map/all_to_all | solution.py:546
  55.0 105.4 %all-gather.3.cloned.1.call-start = ((), (), s32[]{:S(2)}) async-start(), calls=%async_computation.4 | async-start | bytes 4734976 | tf_op jit(solution)/shard_map/all_gather | solution.py:555
  55.0 2.8 %collective-permute-start = (bf16[4,16,512]{2,1,0:T(8,128)(2,1)S(1)}, bf16[4,16,512]{2,1,0:T(8,128)(2,1)S(1)}, u32[]{:S(2)}, u32[]{:S(2)}) collective-permute-start(bf16[4,16,512]{2,1,0:T(8,128)(2,1)S(1)} %slice.3), channel_id=1, source_target_pairs={{0,32},{32,64},{64,96},{96,128},{128,160},{160,192},{192,224},{224... | collective-permute-start | bytes 196616 | tf_op jit(solution)/shard_map/ppermute | solution.py:541
  56.6 15.7 %copy-start.6 = (s32[3]{0:T(128)}, s32[3]{0:T(128)S(1)}, u32[]{:S(2)}) copy-start(s32[3]{0:T(128)S(1)} %pad_add_fusion.ids) | copy-start | bytes 40
  56.6 22.5 %copy-start.12 = (bf16[32,896]{1,0:T(8,128)(2,1)S(1)}, bf16[32,896]{1,0:T(8,128)(2,1)}, u32[]{:S(2)}) copy-start(bf16[32,896]{1,0:T(8,128)(2,1)} %get-tuple-element.29) | copy-start | bytes 172036
  58.7 0.6 copy-start.8
  59.3 11.0 %collective-permute-start.1 = (f32[8,384]{1,0:T(8,128)S(1)}, f32[8,384]{1,0:T(8,128)S(1)}, u32[]{:S(2)}, u32[]{:S(2)}) collective-permute-start(f32[8,384]{1,0:T(8,128)S(1)} %get-tuple-element.33), channel_id=1, source_target_pairs={{0,8},{8,16},{16,24},{24,0},{1,9},{9,17},{17,25},{25,1},{2,10},{10... | collective-permute-start | bytes 36872 | tf_op jit(solution)/shard_map/ppermute | solution.py:525
  62.8 8.0 %collective-permute-start.2 = (f32[8,384]{1,0:T(8,128)S(1)}, f32[8,384]{1,0:T(8,128)S(1)}, u32[]{:S(2)}, u32[]{:S(2)}) collective-permute-start(f32[8,384]{1,0:T(8,128)S(1)} %get-tuple-element.34), channel_id=1, source_target_pairs={{0,16},{8,24},{16,0},{24,8},{1,17},{9,25},{17,1},{25,9},{2,18},{10... | collective-permute-start | bytes 36872 | tf_op jit(solution)/shard_map/ppermute | solution.py:525
  67.4 5.0 %collective-permute-start.3 = (f32[8,384]{1,0:T(8,128)S(1)}, f32[8,384]{1,0:T(8,128)S(1)}, u32[]{:S(2)}, u32[]{:S(2)}) collective-permute-start(f32[8,384]{1,0:T(8,128)S(1)} %get-tuple-element.35), channel_id=1, source_target_pairs={{0,24},{8,0},{16,8},{24,16},{1,25},{9,1},{17,9},{25,17},{2,26},{10... | collective-permute-start | bytes 36872 | tf_op jit(solution)/shard_map/ppermute | solution.py:525
  70.3 2.0 %copy-start.13 = (f32[8,384]{1,0:T(8,128)}, f32[8,384]{1,0:T(8,128)S(1)}, u32[]{:S(2)}) copy-start(f32[8,384]{1,0:T(8,128)S(1)} %collective-permute-done.1.e1) | copy-start | bytes 36868
  70.8 1.5 copy-start.14
  72.3 0.6 copy-start.15
  72.9 34.4 %copy-start.1 = (bf16[4,144,512]{2,1,0:T(8,128)(2,1)S(1)}, bf16[4,144,512]{2,1,0:T(8,128)(2,1)}, u32[]{:S(2)}) copy-start(bf16[4,144,512]{2,1,0:T(8,128)(2,1)} %copy-done) | copy-start | bytes 1769476
  108.7 16.8 %copy-start.2 = (f32[4,4096]{1,0:T(4,128)S(1)}, f32[4,4096]{1,0:T(4,128)}, u32[]{:S(2)}) copy-start(f32[4,4096]{1,0:T(4,128)} %cc_ref.1) | copy-start | bytes 196612
  108.8 16.8 %copy-start.3 = (f32[128,8]{1,0:T(8,128)S(1)}, f32[128,8]{1,0:T(8,128)}, u32[]{:S(2)}) copy-start(f32[128,8]{1,0:T(8,128)} %get-tuple-element.40.cols_ref) | copy-start | bytes 12292
  108.8 16.8 %copy-start.4 = (bf16[128,256]{1,0:T(8,128)(2,1)S(1)}, bf16[128,256]{1,0:T(8,128)(2,1)}, u32[]{:S(2)}) copy-start(bf16[128,256]{1,0:T(8,128)(2,1)} %get-tuple-element.37.xin_ref) | copy-start | bytes 196612
  108.8 16.8 %copy-start.5 = (bf16[128,128]{1,0:T(8,128)(2,1)S(1)}, bf16[128,128]{1,0:T(8,128)(2,1)}, u32[]{:S(2)}) copy-start(bf16[128,128]{1,0:T(8,128)(2,1)} %get-tuple-element.38.bkey_ref) | copy-start | bytes 98308
  108.8 16.8 %copy-start.7 = (s32[3]{0:T(128)S(1)}, s32[3]{0:T(128)}, u32[]{:S(2)}) copy-start(s32[3]{0:T(128)} %copy-done.6) | copy-start | bytes 40
  108.8 16.8 %copy-start.10 = (f32[8,128]{1,0:T(8,128)S(1)}, f32[8,128]{1,0:T(8,128)}, u32[]{:S(2)}) copy-start(f32[8,128]{1,0:T(8,128)} %get-tuple-element.39.rows_ref) | copy-start | bytes 12292
  108.8 51.6 %copy-start.9 = (f32[2048]{0:T(1024)S(1)}, f32[2048]{0:T(1024)}, u32[]{:S(2)}) copy-start(f32[2048]{0:T(1024)} %param.27) | copy-start | bytes 24580
  108.8 51.6 %copy-start.11 = (f32[16]{0:T(128)S(1)}, f32[16]{0:T(128)}, u32[]{:S(2)}) copy-start(f32[16]{0:T(128)} %bias.1) | copy-start | bytes 196
  108.8 16.7 %all-to-all-start.1 = ((f32[4,144,640]{2,1,0:T(8,128)}), f32[4,144,640]{2,1,0:T(8,128)S(1)}, u32[]{:S(2)}, u32[]{:S(2)}) async-start(f32[4,144,640]{2,1,0:T(8,128)} %get-tuple-element.30), calls=%async_computation.1 | async-start | bytes 2949120 | tf_op jit(solution)/shard_map/all_to_all | solution.py:546
  113.4 14.9 %collective-permute-start.4 = (bf16[512,256]{1,0:T(8,128)(2,1)S(1)}, bf16[512,256]{1,0:T(8,128)(2,1)S(1)}, u32[]{:S(2)}, u32[]{:S(2)}) collective-permute-start(bf16[512,256]{1,0:T(8,128)(2,1)S(1)} %get-tuple-element.46.a0), channel_id=1, source_target_pairs={{0,8},{8,16},{16,24},{24,0},{1,9},{9,17},{17,25},{25,1},{2,10},{10... | collective-permute-start | bytes 786440 | tf_op jit(solution)/shard_map/ppermute | solution.py:525
  116.8 14.3 %collective-permute-start.5 = (bf16[512,256]{1,0:T(8,128)(2,1)S(1)}, bf16[512,256]{1,0:T(8,128)(2,1)S(1)}, u32[]{:S(2)}, u32[]{:S(2)}) collective-permute-start(bf16[512,256]{1,0:T(8,128)(2,1)S(1)} %get-tuple-element.46.a0), channel_id=1, source_target_pairs={{0,16},{8,24},{16,0},{24,8},{1,17},{9,25},{17,1},{25,9},{2,18},{10... | collective-permute-start | bytes 786440 | tf_op jit(solution)/shard_map/ppermute | solution.py:525
  121.1 10.0 %collective-permute-start.6 = (bf16[512,256]{1,0:T(8,128)(2,1)S(1)}, bf16[512,256]{1,0:T(8,128)(2,1)S(1)}, u32[]{:S(2)}, u32[]{:S(2)}) collective-permute-start(bf16[512,256]{1,0:T(8,128)(2,1)S(1)} %get-tuple-element.46.a0), channel_id=1, source_target_pairs={{0,24},{8,0},{16,8},{24,16},{1,25},{9,1},{17,9},{25,17},{2,26},{10... | collective-permute-start | bytes 786440 | tf_op jit(solution)/shard_map/ppermute | solution.py:525
Sparse Core Ops, SparseCore 0:
  79.3 81.0 all-gather.2
